TPU v7x, 32 devices: a whole 2x2x4 slice. The times are simulated.
32 devices in a mesh: ep: 8 (over z, x), tp: 4 (over y, core).
Axes of the slice: x: 2, y: 2, z: 4, core: 2. Of those that a mesh axis runs over, the one named last changes fastest.
Arguments:
- mixer_rows: bfloat16 [1024, 2048], P('ep'), may hold values from -40 to 40
- mixer_gain: float32 [2048], replicated, may hold values from 0.1 to 1.9
- inner_weight: bfloat16 [2048, 1024], P(None, 'tp'), may hold values from -0.125 to 0.125
- gate_in_weight: bfloat16 [2048, 1024], P(None, 'tp'), may hold values from -0.125 to 0.125
- gate_out_weight: bfloat16 [2048, 1024], P(None, 'tp'), may hold values from -0.125 to 0.125
- conv_taps: float32 [3, 1024], P(None, 'tp'), may hold values from -3.5 to 3.5
- mixer_out_weight: bfloat16 [1024, 2048], P('tp'), may hold values from -0.1875 to 0.1875
- routed_rows: bfloat16 [2048, 2048], P('ep'), may hold values from -40 to 40
- routed_gain: float32 [2048], replicated, may hold values from 0.1 to 1.9
- route_ids: int32 [2048, 2], P('ep'), may hold values from 0 to 7, all different within a row; in each aligned block of 256 rows (0 to 255, 256 to 511, ...) at most 128 rows name the same one
- route_weights: float32 [2048, 2], P('ep'), may hold values from 0.25 to 1
- expert_gate: bfloat16 [8, 2048, 2048], P('ep', None, 'tp'), may hold values from -0.125 to 0.125
- expert_up: bfloat16 [8, 2048, 2048], P('ep', None, 'tp'), may hold values from -0.125 to 0.125
- expert_down: bfloat16 [8, 2048, 2048], P('ep', 'tp'), may hold values from -0.125 to 0.125
Outputs:
- mixer_output: bfloat16 [1024, 2048], P('ep')
- routed_output: bfloat16 [2048, 2048], P('ep')
Inputs may be any that keep to these rules, and one draw needn't show every extreme that they name: `route_ids`: within each aligned block of 256 tokens, no expert is named by more than 128 choices, a bound that some block reaches; a token's 2 experts differ.
All inputs are finite; a program needn't handle non-finite values.
Results may differ from a plain program's by a relative error of at most 0.019.
Values may be sent and summed in bfloat16 or wider, within the bound.
A program may use at most 64 MiB of HBM per device.

v0:
```python
import jax
import jax.numpy as jnp
from jax import lax
from jax.sharding import PartitionSpec as P


def shifted(value, axis, steps):
    count = lax.axis_size(axis)
    initial, last = (max(0, -steps), min(count, count - steps))
    return lax.ppermute(value, axis, [(source, source + steps) for source in range(initial, last)])


def rms_scale(row_block, gain_row):
    values = row_block.astype(jnp.float32)
    scaled = values * lax.rsqrt(jnp.mean(values * values, axis=-1, keepdims=True) + 1e-06)
    return (scaled * gain_row).astype(jnp.bfloat16)


def on_device(
    mixer_rows,
    mixer_gain,
    inner_weight,
    gate_in_weight,
    gate_out_weight,
    conv_taps,
    mixer_out_weight,
    routed_rows,
    routed_gain,
    route_ids,
    route_weights,
    expert_gate,
    expert_up,
    expert_down,
):
    normed = rms_scale(mixer_rows, mixer_gain)
    inner_proj = jnp.dot(normed, inner_weight, preferred_element_type=jnp.float32)
    gate_in = jnp.dot(normed, gate_in_weight, preferred_element_type=jnp.float32)
    conv_input = (gate_in * inner_proj).astype(jnp.bfloat16)
    gate_out = jnp.dot(normed, gate_out_weight, preferred_element_type=jnp.float32)
    tap_total = conv_taps.shape[0]
    rim_rows = tap_total - 1
    earlier_rows = shifted(conv_input[conv_input.shape[0] - rim_rows :], "ep", 1)
    extended = jnp.concatenate([earlier_rows, conv_input], axis=0).astype(jnp.float32)
    length = conv_input.shape[0]
    conv_out = jnp.zeros(conv_input.shape, jnp.float32)
    for tap_index in range(tap_total):
        conv_out = conv_out + conv_taps[tap_index] * extended[tap_index : tap_index + length]
    gated_conv = (gate_out * conv_out).astype(jnp.bfloat16)
    mixer_terms = jnp.dot(gated_conv, mixer_out_weight, preferred_element_type=jnp.float32)
    routed_normed = rms_scale(routed_rows, routed_gain)
    experts = lax.axis_size("ep")
    groups = lax.axis_size("tp")
    column = lax.axis_index("tp")
    tok_count, pick_count = route_ids.shape
    model_width = routed_rows.shape[1]
    capacity = 2 * tok_count * pick_count // experts
    share_rows = capacity // groups
    flat_ids = route_ids.reshape(-1)
    onehot = (flat_ids[:, None] == jnp.arange(experts, dtype=jnp.int32)[None, :]).astype(jnp.int32)
    slot_rank = jnp.sum((jnp.cumsum(onehot, axis=0) - onehot) * onehot, axis=1)
    slot_number = slot_rank * experts + flat_ids
    owners = jnp.arange(tok_count * pick_count, dtype=jnp.int32) // pick_count
    matches = slot_number[None, :] == jnp.arange(capacity * experts, dtype=jnp.int32)[:, None]
    token_table = jnp.where(
        jnp.any(matches, axis=1), jnp.sum(jnp.where(matches, owners[None, :], 0), axis=1), tok_count
    )
    padded_rows = jnp.concatenate(
        [routed_normed, jnp.zeros((1, model_width), jnp.bfloat16)], axis=0
    )
    table_share = lax.dynamic_slice_in_dim(
        token_table.reshape(capacity, experts), column * share_rows, share_rows, 0
    )
    outgoing = jnp.take(padded_rows, table_share.reshape(-1), axis=0).reshape(
        share_rows, experts, model_width
    )
    arrived = lax.all_to_all(outgoing, "ep", split_axis=1, concat_axis=1, tiled=True)
    incoming = lax.all_gather(arrived, "tp", axis=0, tiled=True)
    slot_rows = incoming.reshape(capacity * experts, model_width)
    gate_act = jnp.dot(slot_rows, expert_gate[0], preferred_element_type=jnp.float32)
    up_act = jnp.dot(slot_rows, expert_up[0], preferred_element_type=jnp.float32)
    hidden = (jax.nn.silu(gate_act) * up_act).astype(jnp.bfloat16)
    summed = lax.psum_scatter(
        jnp.dot(hidden, expert_down[0], preferred_element_type=jnp.float32).astype(jnp.bfloat16),
        "tp",
        scatter_dimension=0,
        tiled=True,
    )
    returned = lax.all_to_all(
        summed.reshape(share_rows, experts, model_width),
        "ep",
        split_axis=1,
        concat_axis=1,
        tiled=True,
    )
    flat_back = jnp.concatenate(
        [
            returned.reshape(share_rows * experts, model_width),
            jnp.zeros((1, model_width), jnp.bfloat16),
        ],
        axis=0,
    )
    local_slot = jnp.where(
        slot_rank // share_rows == column,
        (slot_rank - column * share_rows) * experts + flat_ids,
        share_rows * experts,
    )
    contrib = (
        jnp.take(flat_back, local_slot, axis=0).astype(jnp.float32)
        * route_weights.reshape(-1)[:, None]
    )
    routed_terms = jnp.sum(contrib.reshape(tok_count, pick_count, model_width), axis=1)
    mixer_total, routed_total = (
        lax.psum(mixer_terms.astype(jnp.bfloat16), "tp").astype(jnp.float32),
        lax.psum(routed_terms.astype(jnp.bfloat16), "tp").astype(jnp.float32),
    )
    return (mixer_total.astype(jnp.bfloat16), routed_total.astype(jnp.bfloat16))


def solution(mesh):
    return jax.shard_map(
        on_device,
        mesh=mesh,
        in_specs=(
            P("ep", None),
            P(),
            P(None, "tp"),
            P(None, "tp"),
            P(None, "tp"),
            P(None, "tp"),
            P("tp", None),
            P("ep", None),
            P(),
            P("ep", None),
            P("ep", None),
            P("ep", None, "tp"),
            P("ep", None, "tp"),
            P("ep", "tp", None),
        ),
        out_specs=(P("ep", None), P("ep", None)),
        check_vma=False,
    )
```

profile of v0, /device:TPU:0, one launch (start us, length us, event | category | flops | bytes accessed | tf_op | source)
XLA Modules:
  0.0 255.2 jit_solution(8111063935972421025)
XLA Ops:
  7.2 1.0 copy.67
  8.5 1.1 reduce-window.6
  9.7 0.2 slice_reduce_fusion
  10.0 0.3 fusion.10
  10.3 0.3 select_reduce_fusion
  10.9 1.5 fusion.4
  12.5 1.0 fusion.6
  13.6 2.3 gather_fusion
  15.9 2.4 copy_select_fusion
  18.4 32.8 %all_to_all.10 = bf16[32,8,2048]{2,0,1:T(8,128)(2,1)S(1)} all-to-all(bf16[32,8,2048]{2,0,1:T(8,128)(2,1)S(1)} %copy_select_fusion), channel_id=1, replica_groups=mesh['ep'=8,'tp'=4] {'ep'}, dimensions={1} | all-to-all | bytes 2097152 | tf_op jit(solution)/shard_map/all_to_all | solution.py:76
  51.2 1.5 copy.77
  52.8 33.6 %all-gather.2.cloned.1.call-done = bf16[128,8,2048]{2,1,0:T(8,128)(2,1)} async-done(((bf16[32,8,2048]{2,1,0:T(8,128)(2,1)}), bf16[128,8,2048]{2,1,0:T(8,128)(2,1)}) %all-gather.2.cloned.1.call-update) | async-done | bytes 4194320 | tf_op jit(solution)/shard_map/all_gather | solution.py:77
  86.4 6.6 %fusion.2 = f32[1024,512]{1,0:T(8,128)} fusion(bf16[128,8,2048]{2,1,0:T(8,128)(2,1)} %all-gather.2.cloned.1.call-done, bf16[1,2048,512]{2,1,0:T(8,128)(2,1)} %param.25), kind=kOutput, calls=%fused_computation.4 | convolution fusion | flops 2147483648 | bytes 8388608 | tf_op jit(solution)/shard_map/dot_general | solution.py:79
  93.0 10.0 %convolution_convert_fusion = bf16[1024,2048]{1,0:T(8,128)(2,1)} fusion(bf16[1,512,2048]{2,1,0:T(8,128)(2,1)S(1)} %copy-done, f32[1024,512]{1,0:T(8,128)} %fusion.2, bf16[1,2048,512]{2,1,0:T(8,128)(2,1)} %param.26, bf16[128,8,2048]{2,1,0:T(8,128)(2,1)} %all-gather.2.cloned.1.call-done), kind=kOutput, calls=%fused_computation.8 | convolution fusion | flops 4300210176 | bytes 14680064 | tf_op jit(solution)/shard_map/dot_general | solution.py:83
  103.0 1.0 copy-done.2
  104.0 0.2 fusion.21
  104.2 43.5 %reduce-scatter.2.cloned.1.call-done = bf16[256,2048]{1,0:T(8,128)(2,1)} async-done(((bf16[1024,2048]{1,0:T(8,128)(2,1)}), bf16[256,2048]{1,0:T(8,128)(2,1)}) %reduce-scatter.2.cloned.1.call-update) | async-done | bytes 1048592 | tf_op jit(solution)/shard_map/reduce_scatter | solution.py:82
  147.7 2.8 %copy.78 = bf16[32,8,2048]{2,0,1:T(8,128)(2,1)} copy(bf16[32,8,2048]{2,1,0:T(8,128)(2,1)} %bitcast.47) | data formatting | bytes 2097152 | tf_op jit(solution)/shard_map/reshape | solution.py:89
  150.5 5.5 %all-to-all-start.1 = ((bf16[32,8,2048]{2,0,1:T(8,128)(2,1)}), bf16[32,8,2048]{2,0,1:T(8,128)(2,1)S(1)}, u32[]{:S(2)}, u32[]{:S(2)}) async-start(bf16[32,8,2048]{2,0,1:T(8,128)(2,1)} %copy.78), calls=%async_computation.2 | async-start | bytes 2097152 | tf_op jit(solution)/shard_map/all_to_all | solution.py:88
  156.1 1.7 fusion.40
  157.9 1.8 fusion.16
  159.7 4.1 %collective-permute-start = (bf16[2,256]{1,0:T(2,128)(2,1)S(1)}, bf16[2,256]{1,0:T(2,128)(2,1)S(1)}, u32[]{:S(2)}, u32[]{:S(2)}) collective-permute-start(bf16[2,256]{1,0:T(2,128)(2,1)S(1)} %slice.40), channel_id=1, source_target_pairs={{0,4},{4,8},{8,12},{12,16},{16,20},{20,24},{24,28},{1,5},{5,9},{9,... | collective-permute-start | bytes 3080 | tf_op jit(solution)/shard_map/ppermute | solution.py:10
  164.5 0.3 collective-permute-done
  164.9 3.3 %convolution_convert_fusion.1 = bf16[128,2048]{1,0:T(8,128)(2,1)} fusion(bf16[256,2048]{1,0:T(8,128)(2,1)} %param.20, bf16[2048,256]{1,0:T(8,128)(2,1)} %param.18, f32[130,256]{1,0:T(8,128)S(1)} %maximum_convert_fusion, f32[256]{0:T(256)S(1)} %bitcast.51, f32[256]{0:T(256)S(1)} %bitcast.52, f32[256]{0:T(256)S(1)} %bitcast.50, bf16[128,2048]{1,0:T(8,128)(2,1)} %param.14, ...), kind=kOutput, calls=%fused_computation.11 | convolution fusion | flops 269975552 | bytes 3550720 | tf_op jit(solution)/shard_map/dot_general | solution.py:49
  168.2 13.5 %all-to-all-done.1 = bf16[32,8,2048]{2,0,1:T(8,128)(2,1)S(1)} async-done(((bf16[32,8,2048]{2,0,1:T(8,128)(2,1)}), bf16[32,8,2048]{2,0,1:T(8,128)(2,1)S(1)}, u32[]{:S(2)}, u32[]{:S(2)}) %all-to-all-start.1) | async-done | bytes 1048608 | tf_op jit(solution)/shard_map/all_to_all | solution.py:88
  181.7 0.6 copy.84
  182.4 3.3 %gather_fusion.1 = bf16[512,2048]{1,0:T(8,128)(2,1)} fusion(bf16[257,2048]{1,0:T(8,128)(2,1)S(1)} %concatenate.11, s32[1024]{0:T(1024)S(1)} %pad_clamp_fusion), kind=kCustom, calls=%fused_computation.1 | custom fusion | bytes 4196352 | tf_op jit(solution)/shard_map/jit(_take)/gather | solution.py:108
  185.7 4.4 %gather.15 = bf16[256,2,2048]{2,1,0:T(2,128)(2,1)} reshape(bf16[512,2048]{1,0:T(8,128)(2,1)} %gather_fusion.1) | data formatting | bytes 4194304 | tf_op jit(solution)/shard_map/jit(_take)/gather | solution.py:108
  190.1 10.8 %multiply_reduce_fusion = bf16[256,2048]{1,0:T(8,128)(2,1)} fusion(bf16[256,2,2048]{2,1,0:T(2,128)(2,1)} %gather.15, pred[256,2]{1,0:T(8,128)(4,1)S(1)} %copy.74, f32[256,2]{1,0:T(8,128)S(1)} %copy.81), kind=kLoop, calls=%fused_computation.6 | loop fusion | flops 3670016 | bytes 3148288 | tf_op jit(solution)/shard_map/reduce_sum | solution.py:111
  201.0 43.5 %all-reduce.5.cloned.1.call-done = (bf16[128,2048]{1,0:T(8,128)(2,1)}, bf16[256,2048]{1,0:T(8,128)(2,1)}) async-done(((bf16[128,2048]{1,0:T(8,128)(2,1)}, bf16[256,2048]{1,0:T(8,128)(2,1)}), (bf16[128,2048]{1,0:T(8,128)(2,1)}, bf16[256,2048]{1,0:T(8,128)(2,1)})) %all-reduce.5.cloned.1.call-update) | async-done | bytes 1572880 | tf_op jit(solution)/shard_map/psum | solution.py:113
  244.5 1.9 copy.87
  246.4 2.3 copy.88
  (48 shorter events, 1.8 us)
Async XLA Ops:
  7.2 85.8 %copy-start = (bf16[1,512,2048]{2,1,0:T(8,128)(2,1)S(1)}, bf16[1,512,2048]{2,1,0:T(8,128)(2,1)}, u32[]{:S(2)}) copy-start(bf16[1,512,2048]{2,1,0:T(8,128)(2,1)} %param.27) | copy-start | bytes 6291460
  7.2 5.3 %copy-start.1 = (bf16[256,2048]{1,0:T(8,128)(2,1)S(1)}, bf16[256,2048]{1,0:T(8,128)(2,1)}, u32[]{:S(2)}) copy-start(bf16[256,2048]{1,0:T(8,128)(2,1)} %param.21) | copy-start | bytes 3145732
  7.2 79.2 %all-gather.2.cloned.1.call-start = ((), (), s32[]{:S(2)}) async-start(), calls=%async_computation.3 | async-start | bytes 5242880 | tf_op jit(solution)/shard_map/all_gather | solution.py:77
  52.8 95.0 %reduce-scatter.2.cloned.1.call-start = ((), (), s32[]{:S(2)}) async-start(), calls=%async_computation.4 | async-start | bytes 5242880 | tf_op jit(solution)/shard_map/reduce_scatter | solution.py:82
  103.0 1.0 copy-start.2
  147.7 8.4 %copy-start.3 = (f32[2048]{0:T(1024)S(1)}, f32[2048]{0:T(1024)}, u32[]{:S(2)}) copy-start(f32[2048]{0:T(1024)} %param.15) | copy-start | bytes 24580
  150.5 31.2 %all-to-all-start.1 = ((bf16[32,8,2048]{2,0,1:T(8,128)(2,1)}), bf16[32,8,2048]{2,0,1:T(8,128)(2,1)S(1)}, u32[]{:S(2)}, u32[]{:S(2)}) async-start(bf16[32,8,2048]{2,0,1:T(8,128)(2,1)} %copy.78), calls=%async_computation.2 | async-start | bytes 2097152 | tf_op jit(solution)/shard_map/all_to_all | solution.py:88
  156.0 8.1 %copy-start.4 = (s32[256,2]{0,1:T(2,128)S(1)}, s32[256,2]{0,1:T(2,128)}, u32[]{:S(2)}) copy-start(s32[256,2]{0,1:T(2,128)} %param.23) | copy-start | bytes 6148
  156.0 8.1 %copy-start.5 = (f32[3,256]{1,0:T(4,128)S(1)}, f32[3,256]{1,0:T(4,128)}, u32[]{:S(2)}) copy-start(f32[3,256]{1,0:T(4,128)} %param.19) | copy-start | bytes 9220
  156.0 88.4 %all-reduce.5.cloned.1.call-start = ((), (), s32[]{:S(2)}) async-start(), calls=%async_computation.5 | async-start | bytes 3145728 | tf_op jit(solution)/shard_map/psum | solution.py:113
  156.1 8.3 %copy-start.6 = (f32[256,2]{0,1:T(2,128)S(1)}, f32[256,2]{0,1:T(2,128)}, u32[]{:S(2)}) copy-start(f32[256,2]{0,1:T(2,128)} %param.24) | copy-start | bytes 6148
  159.7 5.2 %collective-permute-start = (bf16[2,256]{1,0:T(2,128)(2,1)S(1)}, bf16[2,256]{1,0:T(2,128)(2,1)S(1)}, u32[]{:S(2)}, u32[]{:S(2)}) collective-permute-start(bf16[2,256]{1,0:T(2,128)(2,1)S(1)} %slice.40), channel_id=1, source_target_pairs={{0,4},{4,8},{8,12},{12,16},{16,20},{20,24},{24,28},{1,5},{5,9},{9,... | collective-permute-start | bytes 3080 | tf_op jit(solution)/shard_map/ppermute | solution.py:10
Sparse Core Ops, SparseCore 0:
  52.9 33.4 all-gather.1
  103.1 44.5 reduce-scatter.1
  201.1 43.3 all-reduce.4
where the time goes:
time: 256 us; the launch traced here: 255 us
  waiting for transfers between devices  134 us (52%)
  blocking collectives  32.8 us (13%)
  matrix products  23.4 us (9%)
  local copies, waits for them, and re-layouts  22.8 us (9%)
  other arithmetic  18 us (7%)
  between operations  14 us (5%)
  starting transfers between devices  9.73 us (4%)
    reduce_scatter x1, waiting for transfers between devices, on_device(): lax.psum_scatter(jnp.dot(hidden, expert_down[0], preferred_element_type=j...  43.5 us
    psum x1, waiting for transfers between devices, on_device(): lax.psum(mixer_terms.astype(jnp.bfloat16), 'tp').astype(jnp.float32)  43.5 us
    all_gather x1, waiting for transfers between devices, on_device(): incoming = lax.all_gather(arrived, 'tp', axis=0, tiled=True)  33.6 us
    all_to_all x1, blocking collectives, on_device(): lax.all_to_all(outgoing, 'ep', split_axis=1, concat_axis=1, tiled=True)  32.8 us
    all_to_all x1, waiting for transfers between devices, on_device(): lax.all_to_all(summed.reshape(share_rows, experts, model_width), 'ep', sp...  13.5 us
    reduce_sum x1, other arithmetic, on_device(): jnp.sum(contrib.reshape(tok_count, pick_count, model_width), axis=1)  10.8 us
    dot_general x1, matrix products, on_device(): jnp.dot(hidden, expert_down[0], preferred_element_type=jnp.float32)  9.96 us
    gather x2, local copies, waits for them, and re-layouts, on_device(): jnp.take(flat_back, local_slot, axis=0).astype(jnp.float32)  7.75 us
  transfers between devices with their start and end apart: 5, of which 5 were waited for; matrix products, arithmetic and copies ran while one was open for 3% of the time, Pallas kernels for 0%

commit v1 on v0

--- a/solution.py
+++ b/solution.py
@@ -2,6 +2,12 @@
 import jax.numpy as jnp
 from jax import lax
 from jax.sharding import PartitionSpec as P
+
+
+def add_all(x, axis):
+    pieces = lax.all_gather(x, axis, axis=0, tiled=False)
+    total = pieces.sum(axis=0)
+    return total
 
 
 def shifted(value, axis, steps):
@@ -110,7 +116,7 @@
     )
     routed_terms = jnp.sum(contrib.reshape(tok_count, pick_count, model_width), axis=1)
     mixer_total, routed_total = (
-        lax.psum(mixer_terms.astype(jnp.bfloat16), "tp").astype(jnp.float32),
+        add_all(mixer_terms.astype(jnp.bfloat16), "tp").astype(jnp.float32),
         lax.psum(routed_terms.astype(jnp.bfloat16), "tp").astype(jnp.float32),
     )
     return (mixer_total.astype(jnp.bfloat16), routed_total.astype(jnp.bfloat16))

time: 256 us -> 245 us (0.957)
  waiting for transfers between devices: 134 us -> 124 us
  other arithmetic: 18 us -> 20.9 us
    psum x1, waiting for transfers between devices: 43.5 us -> 31.5 us  [on_device(): lax.psum(routed_terms.astype(jnp.bfloat16), 'tp').astype(jnp.float32)]
    all_to_all x1, waiting for transfers between devices: 13.5 us -> 24.8 us  [on_device(): lax.all_to_all(summed.reshape(share_rows, experts, model_width), 'ep', sp...]
    reduce_scatter x1, waiting for transfers between devices: 43.5 us -> 33 us  [on_device(): lax.psum_scatter(jnp.dot(hidden, expert_down[0], preferred_element_type=j...]
    reduce_sum x0 -> x1, other arithmetic: none -> 2.92 us  [add_all(): total = pieces.sum(axis=0)]
    unnamed x18 -> x19, local copies, waits for them, and re-layouts: 6.36 us -> 4.41 us
  transfers between devices with their start and end apart: 5 -> 6, of which waited for: 5 -> 5; matrix products, arithmetic and copies ran while one was open for 3% -> 13% of each run, Pallas kernels for 0% -> 0%
where the time goes in v1:
time: 245 us; the launch traced here: 244 us
  waiting for transfers between devices  124 us (51%)
  blocking collectives  32.8 us (13%)
  matrix products  22.3 us (9%)
  local copies, waits for them, and re-layouts  20.9 us (9%)
  other arithmetic  20.9 us (9%)
  between operations  14 us (6%)
  starting transfers between devices  9.05 us (4%)
    all_gather x1, waiting for transfers between devices, on_device(): incoming = lax.all_gather(arrived, 'tp', axis=0, tiled=True)  33.6 us
    reduce_scatter x1, waiting for transfers between devices, on_device(): lax.psum_scatter(jnp.dot(hidden, expert_down[0], preferred_element_type=j...  33 us
    all_to_all x1, blocking collectives, on_device(): lax.all_to_all(outgoing, 'ep', split_axis=1, concat_axis=1, tiled=True)  32.8 us
    psum x1, waiting for transfers between devices, on_device(): lax.psum(routed_terms.astype(jnp.bfloat16), 'tp').astype(jnp.float32)  31.5 us
    all_to_all x1, waiting for transfers between devices, on_device(): lax.all_to_all(summed.reshape(share_rows, experts, model_width), 'ep', sp...  24.8 us
    reduce_sum x1, other arithmetic, on_device(): jnp.sum(contrib.reshape(tok_count, pick_count, model_width), axis=1)  10.8 us
    dot_general x1, matrix products, on_device(): jnp.dot(hidden, expert_down[0], preferred_element_type=jnp.float32)  9.96 us
    gather x2, local copies, waits for them, and re-layouts, on_device(): jnp.take(flat_back, local_slot, axis=0).astype(jnp.float32)  7.75 us
  transfers between devices with their start and end apart: 6, of which 5 were waited for; matrix products, arithmetic and copies ran while one was open for 13% of the time, Pallas kernels for 0%

profile of v1, /device:TPU:0, one launch (start us, length us, event | category | flops | bytes accessed | tf_op | source)
XLA Modules:
  0.0 244.3 jit_solution(13137648703598323531)
XLA Ops:
  7.2 1.0 copy.67
  8.5 1.1 reduce-window.6
  9.7 0.2 slice_reduce_fusion
  10.0 0.3 fusion.10
  10.3 0.3 select_reduce_fusion
  10.9 1.5 fusion.4
  12.5 1.0 fusion.6
  13.6 2.3 gather_fusion
  15.9 2.4 %copy_select_fusion = bf16[32,8,2048]{2,0,1:T(8,128)(2,1)S(1)} fusion(bf16[32,8,2048]{2,1,0:T(8,128)(2,1)} %bitcast.46, pred[32,8]{0,1:T(8,128)(4,1)S(1)} %copy.75), kind=kLoop, calls=%fused_computation.32 | loop fusion | flops 524288 | bytes 2097408 | tf_op jit(solution)/shard_map/jit(_take)/select_n | solution.py:79
  18.4 32.8 %all_to_all.10 = bf16[32,8,2048]{2,0,1:T(8,128)(2,1)S(1)} all-to-all(bf16[32,8,2048]{2,0,1:T(8,128)(2,1)S(1)} %copy_select_fusion), channel_id=1, replica_groups=mesh['ep'=8,'tp'=4] {'ep'}, dimensions={1} | all-to-all | bytes 2097152 | tf_op jit(solution)/shard_map/all_to_all | solution.py:82
  51.2 1.5 copy.77
  52.8 33.6 %all-gather.4.cloned.1.call-done = bf16[128,8,2048]{2,1,0:T(8,128)(2,1)} async-done(((bf16[32,8,2048]{2,1,0:T(8,128)(2,1)}), bf16[128,8,2048]{2,1,0:T(8,128)(2,1)}) %all-gather.4.cloned.1.call-update) | async-done | bytes 4194320 | tf_op jit(solution)/shard_map/all_gather | solution.py:83
  86.4 6.6 %fusion.2 = f32[1024,512]{1,0:T(8,128)} fusion(bf16[128,8,2048]{2,1,0:T(8,128)(2,1)} %all-gather.4.cloned.1.call-done, bf16[1,2048,512]{2,1,0:T(8,128)(2,1)} %param.25), kind=kOutput, calls=%fused_computation.4 | convolution fusion | flops 2147483648 | bytes 8388608 | tf_op jit(solution)/shard_map/dot_general | solution.py:85
  93.0 10.0 %convolution_convert_fusion = bf16[1024,2048]{1,0:T(8,128)(2,1)} fusion(bf16[1,512,2048]{2,1,0:T(8,128)(2,1)S(1)} %copy-done, f32[1024,512]{1,0:T(8,128)} %fusion.2, bf16[1,2048,512]{2,1,0:T(8,128)(2,1)} %param.26, bf16[128,8,2048]{2,1,0:T(8,128)(2,1)} %all-gather.4.cloned.1.call-done), kind=kOutput, calls=%fused_computation.8 | convolution fusion | flops 4300210176 | bytes 14680064 | tf_op jit(solution)/shard_map/dot_general | solution.py:89
  103.1 1.0 copy-done.2
  104.0 0.2 fusion.21
  104.2 1.7 fusion.40
  105.9 0.4 fusion.16
  106.3 3.4 %collective-permute-start = (bf16[2,256]{1,0:T(2,128)(2,1)S(1)}, bf16[2,256]{1,0:T(2,128)(2,1)S(1)}, u32[]{:S(2)}, u32[]{:S(2)}) collective-permute-start(bf16[2,256]{1,0:T(2,128)(2,1)S(1)} %slice.40), channel_id=1, source_target_pairs={{0,4},{4,8},{8,12},{12,16},{16,20},{20,24},{24,28},{1,5},{5,9},{9,... | collective-permute-start | bytes 3080 | tf_op jit(solution)/shard_map/ppermute | solution.py:16
  109.7 1.3 collective-permute-done
  111.0 3.7 %convolution_convert_fusion.1 = bf16[128,2048]{1,0:T(8,128)(2,1)} fusion(bf16[256,2048]{1,0:T(8,128)(2,1)} %param.20, bf16[2048,256]{1,0:T(8,128)(2,1)} %param.18, f32[130,256]{1,0:T(8,128)S(1)} %maximum_convert_fusion, f32[256]{0:T(256)S(1)} %bitcast.53, f32[256]{0:T(256)S(1)} %bitcast.54, f32[256]{0:T(256)S(1)} %bitcast.52, ...), kind=kOutput, calls=%fused_computation.11 | convolution fusion | flops 269975552 | bytes 3550720 | tf_op jit(solution)/shard_map/dot_general | solution.py:55
  114.7 33.0 %reduce-scatter.2.cloned.1.call-done = bf16[256,2048]{1,0:T(8,128)(2,1)} async-done(((bf16[1024,2048]{1,0:T(8,128)(2,1)}), bf16[256,2048]{1,0:T(8,128)(2,1)}) %reduce-scatter.2.cloned.1.call-update) | async-done | bytes 1048592 | tf_op jit(solution)/shard_map/reduce_scatter | solution.py:88
  147.7 2.8 %copy.78 = bf16[32,8,2048]{2,0,1:T(8,128)(2,1)} copy(bf16[32,8,2048]{2,1,0:T(8,128)(2,1)} %bitcast.49) | data formatting | bytes 2097152 | tf_op jit(solution)/shard_map/reshape | solution.py:95
  150.5 5.5 %all-to-all-start.1 = ((bf16[32,8,2048]{2,0,1:T(8,128)(2,1)}), bf16[32,8,2048]{2,0,1:T(8,128)(2,1)S(1)}, u32[]{:S(2)}, u32[]{:S(2)}) async-start(bf16[32,8,2048]{2,0,1:T(8,128)(2,1)} %copy.78), calls=%async_computation.2 | async-start | bytes 2097152 | tf_op jit(solution)/shard_map/all_to_all | solution.py:94
  156.9 24.8 %all-to-all-done.1 = bf16[32,8,2048]{2,0,1:T(8,128)(2,1)S(1)} async-done(((bf16[32,8,2048]{2,0,1:T(8,128)(2,1)}), bf16[32,8,2048]{2,0,1:T(8,128)(2,1)S(1)}, u32[]{:S(2)}, u32[]{:S(2)}) %all-to-all-start.1) | async-done | bytes 1048608 | tf_op jit(solution)/shard_map/all_to_all | solution.py:94
  181.7 0.6 copy.84
  182.4 3.3 %gather_fusion.1 = bf16[512,2048]{1,0:T(8,128)(2,1)} fusion(bf16[257,2048]{1,0:T(8,128)(2,1)S(1)} %concatenate.11, s32[1024]{0:T(1024)S(1)} %pad_clamp_fusion), kind=kCustom, calls=%fused_computation.1 | custom fusion | bytes 4196352 | tf_op jit(solution)/shard_map/jit(_take)/gather | solution.py:114
  185.7 4.4 %gather.15 = bf16[256,2,2048]{2,1,0:T(2,128)(2,1)} reshape(bf16[512,2048]{1,0:T(8,128)(2,1)} %gather_fusion.1) | data formatting | bytes 4194304 | tf_op jit(solution)/shard_map/jit(_take)/gather | solution.py:114
  190.1 10.8 %multiply_reduce_fusion = bf16[256,2048]{1,0:T(8,128)(2,1)} fusion(bf16[256,2,2048]{2,1,0:T(2,128)(2,1)} %gather.15, pred[256,2]{1,0:T(8,128)(4,1)S(1)} %copy.74, f32[256,2]{1,0:T(8,128)S(1)} %copy.81), kind=kLoop, calls=%fused_computation.6 | loop fusion | flops 3670016 | bytes 3148288 | tf_op jit(solution)/shard_map/reduce_sum | solution.py:117
  201.0 2.9 %reduce_sum.62 = bf16[128,2048]{1,0:T(8,128)(2,1)} reduce(bf16[4,128,2048]{2,1,0:T(8,128)(2,1)} %bitcast.48, bf16[]{:T(256)} %constant.72.clone.1), dimensions={0}, to_apply=%region_1.0 | reduce | flops 786432 | bytes 2621442 | tf_op jit(solution)/shard_map/reduce_sum | solution.py:9
  203.9 31.5 %all-reduce.4.cloned.1.call-done = bf16[256,2048]{1,0:T(8,128)(2,1)} async-done(((bf16[256,2048]{1,0:T(8,128)(2,1)}), bf16[256,2048]{1,0:T(8,128)(2,1)}) %all-reduce.4.cloned.1.call-update) | async-done | bytes 1048592 | tf_op jit(solution)/shard_map/psum | solution.py:120
  235.5 2.3 copy.86
  (53 shorter events, 1.9 us)
Async XLA Ops:
  7.2 85.8 %copy-start = (bf16[1,512,2048]{2,1,0:T(8,128)(2,1)S(1)}, bf16[1,512,2048]{2,1,0:T(8,128)(2,1)}, u32[]{:S(2)}) copy-start(bf16[1,512,2048]{2,1,0:T(8,128)(2,1)} %param.27) | copy-start | bytes 6291460
  7.2 5.3 %copy-start.1 = (bf16[256,2048]{1,0:T(8,128)(2,1)S(1)}, bf16[256,2048]{1,0:T(8,128)(2,1)}, u32[]{:S(2)}) copy-start(bf16[256,2048]{1,0:T(8,128)(2,1)} %param.21) | copy-start | bytes 3145732
  7.2 79.2 %all-gather.4.cloned.1.call-start = ((), (), s32[]{:S(2)}) async-start(), calls=%async_computation.3 | async-start | bytes 5242880 | tf_op jit(solution)/shard_map/all_gather | solution.py:83
  52.8 95.0 %reduce-scatter.2.cloned.1.call-start = ((), (), s32[]{:S(2)}) async-start(), calls=%async_computation.4 | async-start | bytes 5242880 | tf_op jit(solution)/shard_map/reduce_scatter | solution.py:88
  103.0 1.0 copy-start.2
  103.0 1.2 copy-start.3
  103.0 6.7 %copy-start.5 = (f32[3,256]{1,0:T(4,128)S(1)}, f32[3,256]{1,0:T(4,128)}, u32[]{:S(2)}) copy-start(f32[3,256]{1,0:T(4,128)} %param.19) | copy-start | bytes 9220
  103.0 98.0 %all-gather.6.cloned.1.call-start = ((), (), s32[]{:S(2)}) async-start(), calls=%async_computation.6 | async-start | bytes 2621440 | tf_op jit(solution)/shard_map/all_gather | solution.py:8
  104.0 1.9 copy-start.7
  106.3 4.7 %collective-permute-start = (bf16[2,256]{1,0:T(2,128)(2,1)S(1)}, bf16[2,256]{1,0:T(2,128)(2,1)S(1)}, u32[]{:S(2)}, u32[]{:S(2)}) collective-permute-start(bf16[2,256]{1,0:T(2,128)(2,1)S(1)} %slice.40), channel_id=1, source_target_pairs={{0,4},{4,8},{8,12},{12,16},{16,20},{20,24},{24,28},{1,5},{5,9},{9,... | collective-permute-start | bytes 3080 | tf_op jit(solution)/shard_map/ppermute | solution.py:16
  147.7 8.7 %copy-start.4 = (s32[256,2]{0,1:T(2,128)S(1)}, s32[256,2]{0,1:T(2,128)}, u32[]{:S(2)}) copy-start(s32[256,2]{0,1:T(2,128)} %param.23) | copy-start | bytes 6148
  147.7 8.9 %copy-start.6 = (f32[256,2]{0,1:T(2,128)S(1)}, f32[256,2]{0,1:T(2,128)}, u32[]{:S(2)}) copy-start(f32[256,2]{0,1:T(2,128)} %param.24) | copy-start | bytes 6148
  150.5 31.2 %all-to-all-start.1 = ((bf16[32,8,2048]{2,0,1:T(8,128)(2,1)}), bf16[32,8,2048]{2,0,1:T(8,128)(2,1)S(1)}, u32[]{:S(2)}, u32[]{:S(2)}) async-start(bf16[32,8,2048]{2,0,1:T(8,128)(2,1)} %copy.78), calls=%async_computation.2 | async-start | bytes 2097152 | tf_op jit(solution)/shard_map/all_to_all | solution.py:94
  156.1 79.4 %all-reduce.4.cloned.1.call-start = ((), (), s32[]{:S(2)}) async-start(), calls=%async_computation.5 | async-start | bytes 2097152 | tf_op jit(solution)/shard_map/psum | solution.py:120
Sparse Core Ops, SparseCore 0:
  52.9 33.4 all-gather.3
  103.1 44.5 reduce-scatter.1
  149.9 22.5 all-gather.5
  201.1 34.3 all-reduce.3
